TPU v7x, 512 devices: a 8x2x16 block of a 8x8x16 slice. The times are simulated.
512 devices in a mesh: grp: 2 (over y), sp: 16 (over z), tp: 16 (over x, core).
Axes of the slice: x: 8, y: 2, z: 16, core: 2. Of those that a mesh axis runs over, the one named last changes fastest.
The devices are a block of a 8x8x16 slice.
Arguments:
- target: bfloat16 [4096, 2048], P(('grp', 'sp', 'tp')), parts along dimension 0, may hold values from -5 to 5
- source: bfloat16 [32768, 2048], P(('grp', 'sp', 'tp')), parts along dimension 0, may hold values from -5 to 5
- source_gain: float32 [2048], replicated, may hold values from 0.1 to 1.9
- pre_first: float32 [2048], replicated, may hold values from 0.1 to 1.9
- query_first: bfloat16 [2048, 2048], P(None, 'tp')
- keyval_first: bfloat16 [2048, 1024], P(None, 'tp')
- out_first: bfloat16 [2048, 2048], P('tp'), may hold values from -0.125 to 0.125
- post_first: float32 [2048], replicated, may hold values from 0.1 to 1.9
- ffn_pre: float32 [2048], replicated, may hold values from 0.1 to 1.9
- w_gate: bfloat16 [2048, 2816], P(None, 'tp'), may hold values from -0.125 to 0.125
- w_value: bfloat16 [2048, 2816], P(None, 'tp'), may hold values from -0.125 to 0.125
- conv_gate: float32 [3, 2816], P(None, 'tp'), may hold values from -3.5 to 3.5
- conv_value: float32 [3, 2816], P(None, 'tp'), may hold values from -3.5 to 3.5
- w_down: bfloat16 [2816, 2048], P('tp'), may hold values from -0.109375 to 0.109375
- ffn_post: float32 [2048], replicated, may hold values from 0.1 to 1.9
- pre_second: float32 [2048], replicated, may hold values from 0.1 to 1.9
- query_second: bfloat16 [2048, 2048], P(None, 'tp')
- keyval_second: bfloat16 [2048, 1024], P(None, 'tp')
- out_second: bfloat16 [2048, 2048], P('tp'), may hold values from -0.125 to 0.125
- post_second: float32 [2048], replicated, may hold values from 0.1 to 1.9
Outputs:
- decoded: float32 [4096, 2048], P(('grp', 'sp', 'tp')), parts along dimension 0
There are 2 independent parts, one for each index of `grp`. A program takes and returns all parts, laid end to end along the dimension named above; an argument that names none is the same for every part. Nothing has to cross between parts.
All inputs are finite; a program needn't handle non-finite values.
Results may differ from a plain program's by a relative error of at most 0.04.
Values may be sent and summed in bfloat16 or wider, within the bound.
A program may use at most 128 MiB of HBM per device.

v0:
```python
import jax
import jax.numpy as jnp
from jax import lax
from jax.sharding import PartitionSpec as P

HEAD = 128
KVH = 4


def in_blocks(array, dim, size):
    before, after = (array.shape[:dim], array.shape[dim + 1 :])
    return jnp.moveaxis(array.reshape(*before, size, -1, *after), dim, 0)


def sent_and_summed(array, axis, dim):
    parts = in_blocks(array, dim, lax.axis_size(axis))
    arrived = lax.all_to_all(parts, axis, split_axis=0, concat_axis=0, tiled=True)
    return arrived.astype(jnp.float32).sum(axis=0)


def swapped(block, axis, distance):
    count = lax.axis_size(axis)
    route = []
    for low in range(count):
        high = low | 1 << distance
        if high != low and high < count:
            route += [(low, high), (high, low)]
    return lax.ppermute(block, axis, route)


def in_one_piece(arrays, axis, dim, along):
    both = jnp.concatenate(arrays, axis=along)
    result, at, done = (lax.all_gather(both, axis, axis=dim, tiled=True), 0, [])
    for a in arrays:
        done.append(lax.slice_in_dim(result, at, at + a.shape[along], axis=along))
        at += a.shape[along]
    return tuple(done)


def shifted(value, axis, steps):
    count = lax.axis_size(axis)
    leading, last = (max(0, -steps), min(count, count - steps))
    return lax.ppermute(value, axis, [(source, source + steps) for source in range(leading, last)])


def normed(values, gain):
    widened = values.astype(jnp.float32)
    return widened * lax.rsqrt(jnp.mean(widened * widened, axis=-1, keepdims=True) + 1e-06) * gain


def project_rows(rows_here, weights):
    shard_rows = lax.all_gather(rows_here, "tp", axis=0, tiled=True)
    products = [
        jnp.dot(shard_rows, weight, preferred_element_type=jnp.float32).astype(jnp.bfloat16)
        for weight in weights
    ]
    return jnp.concatenate(products, axis=1)


def summed_rows(parts, weight):
    return sent_and_summed(
        jnp.dot(parts, weight, preferred_element_type=jnp.float32).astype(jnp.bfloat16), "tp", 0
    )


def key_columns(source_rows, keyval_first, keyval_second):
    both_layers = jnp.concatenate([keyval_first, keyval_second], axis=1)
    columns = jnp.einsum(
        "rd,dc->cr",
        lax.all_gather(source_rows, "tp", axis=0, tiled=True),
        both_layers,
        preferred_element_type=jnp.float32,
    ).astype(jnp.bfloat16)
    column_count = keyval_first.shape[1]
    stacked = columns.reshape(2, column_count, columns.shape[1])
    own_index = lax.axis_index("tp")
    doublings = (2 * HEAD // column_count).bit_length() - 1
    for bit_number in range(doublings):
        lower_half = own_index // 2**bit_number % 2 == 0
        half_rows = stacked.shape[2] // 2
        outgoing = jnp.where(lower_half, stacked[:, :, half_rows:], stacked[:, :, :half_rows])
        retained = jnp.where(lower_half, stacked[:, :, :half_rows], stacked[:, :, half_rows:])
        partner = swapped(outgoing, "tp", bit_number)
        stacked = jnp.where(
            lower_half,
            jnp.concatenate([retained, partner], axis=1),
            jnp.concatenate([partner, retained], axis=1),
        )
    return (stacked[:, :HEAD], stacked[:, HEAD:])


def absorber(query_heads, running, shard_pair):
    scale_factor = HEAD ** (-0.5)
    best_score, weight_sum, weighted = running
    key_block, value_block = shard_pair
    scores = (
        jnp.einsum("thd,ds->ths", query_heads, key_block, preferred_element_type=jnp.float32)
        * scale_factor
    )
    newest = jnp.max(scores, axis=2)
    rescale = jnp.exp(best_score - newest)
    weights = jnp.exp(scores - newest[:, :, None])
    weight_sum = weight_sum * rescale + jnp.sum(weights, axis=2)
    weighted = weighted * rescale[:, :, None] + jnp.einsum(
        "ths,ds->thd", weights.astype(jnp.bfloat16), value_block, preferred_element_type=jnp.float32
    )
    return (newest, weight_sum, weighted)


def empty_running(row_count, head_count):
    return (
        jnp.full((row_count, head_count), -jnp.inf, jnp.float32),
        jnp.zeros((row_count, head_count), jnp.float32),
        jnp.zeros((row_count, head_count, HEAD), jnp.float32),
    )


def attend_shares(queries, keys_t, values_t):
    row_count = queries.shape[0]
    own_heads = queries.shape[1] // HEAD
    group_count = lax.axis_size("tp") // KVH
    doublings = group_count.bit_length() - 1
    own_index = lax.axis_index("tp")
    grouped = queries
    for bit_number in range(doublings):
        lower_half = own_index // 2**bit_number % 2 == 0
        partner = swapped(grouped, "tp", bit_number)
        grouped = jnp.where(
            lower_half,
            jnp.concatenate([grouped, partner], axis=1),
            jnp.concatenate([partner, grouped], axis=1),
        )
    head_count = grouped.shape[1] // HEAD
    query_heads = grouped.reshape(row_count, head_count, HEAD)
    best_score, weight_sum, weighted = absorber(
        query_heads,
        empty_running(row_count, head_count),
        in_one_piece((keys_t, values_t), "sp", 1, 0),
    )
    for bit_number in range(doublings):
        other_best, other_sum, other_weighted = (
            swapped(best_score.astype(jnp.bfloat16), "tp", bit_number).astype(best_score.dtype),
            swapped(weight_sum.astype(jnp.bfloat16), "tp", bit_number).astype(weight_sum.dtype),
            swapped(weighted.astype(jnp.bfloat16), "tp", bit_number).astype(weighted.dtype),
        )
        newest = jnp.maximum(best_score, other_best)
        own_scale = jnp.exp(best_score - newest)
        other_scale = jnp.exp(other_best - newest)
        weight_sum = weight_sum * own_scale + other_sum * other_scale
        weighted = weighted * own_scale[:, :, None] + other_weighted * other_scale[:, :, None]
        best_score = newest
    first_head = own_index % group_count * own_heads
    chosen = lax.dynamic_slice_in_dim(weighted, first_head, own_heads, 1)
    chosen_sums = lax.dynamic_slice_in_dim(weight_sum, first_head, own_heads, 1)
    return (
        (chosen / chosen_sums[:, :, None]).reshape(row_count, own_heads * HEAD).astype(jnp.bfloat16)
    )


def causal_mix(rim_rows, up_rows, conv_taps):
    padded = jnp.concatenate([rim_rows, up_rows], axis=0).astype(jnp.float32)
    length = up_rows.shape[0]
    return (
        conv_taps[0] * padded[:length]
        + conv_taps[1] * padded[1 : length + 1]
        + conv_taps[2] * padded[2:]
    )


def per_device(
    target,
    source,
    source_gain,
    pre_first,
    query_first,
    keyval_first,
    out_first,
    post_first,
    ffn_pre,
    w_gate,
    w_value,
    conv_gate,
    conv_value,
    w_down,
    ffn_post,
    pre_second,
    query_second,
    keyval_second,
    out_second,
    post_second,
):
    source_rows = normed(source, source_gain).astype(jnp.bfloat16)
    keys_t, values_t = key_columns(source_rows, keyval_first, keyval_second)

    def attention_layer(stream, pre_gain, w_query, layer_index, w_out, post_gain):
        queries = project_rows(normed(stream, pre_gain).astype(jnp.bfloat16), (w_query,))
        heads = attend_shares(queries, keys_t[layer_index], values_t[layer_index])
        mixed = summed_rows(heads, w_out)
        return stream.astype(jnp.float32) + normed(mixed, post_gain)

    after_first = attention_layer(target, pre_first, query_first, 0, out_first, post_first)
    up_both = project_rows(normed(after_first, ffn_pre).astype(jnp.bfloat16), (w_gate, w_value))
    hidden_width = w_gate.shape[1]
    up_gate = up_both[:, :hidden_width]
    up_value = up_both[:, hidden_width:]
    rim_gate, rim_value = shifted((up_gate[-2:], up_value[-2:]), "sp", 1)
    gated = (
        jax.nn.gelu(causal_mix(rim_gate, up_gate, conv_gate), approximate=True)
        * causal_mix(rim_value, up_value, conv_value)
    ).astype(jnp.bfloat16)
    ffn_sum = summed_rows(gated, w_down)
    after_ffn = after_first + normed(ffn_sum, ffn_post)
    return attention_layer(after_ffn, pre_second, query_second, 1, out_second, post_second)


def solution(mesh):
    placed = (
        P(("grp", "sp", "tp"), None),
        P(("grp", "sp", "tp"), None),
        P(),
        P(),
        P(None, "tp"),
        P(None, "tp"),
        P("tp", None),
        P(),
        P(),
        P(None, "tp"),
        P(None, "tp"),
        P(None, "tp"),
        P(None, "tp"),
        P("tp", None),
        P(),
        P(),
        P(None, "tp"),
        P(None, "tp"),
        P("tp", None),
        P(),
    )
    return jax.shard_map(
        per_device,
        mesh=mesh,
        in_specs=placed,
        out_specs=P(("grp", "sp", "tp"), None),
        check_vma=False,
    )
```

profile of v0, /device:TPU:65, one launch (start us, length us, event | category | flops | bytes accessed | tf_op | source)
XLA Modules:
  0.0 380.8 jit_solution(5917875736320434852)
XLA Ops:
  6.6 1.2 fusion.19
  7.8 1.8 fusion.21
  9.8 83.2 %all-gather.4.cloned.1.call-done = bf16[1024,2048]{1,0:T(8,128)(2,1)} async-done(((bf16[64,2048]{1,0:T(8,128)(2,1)}), bf16[1024,2048]{1,0:T(8,128)(2,1)}) %all-gather.4.cloned.1.call-update) | async-done | bytes 4194320 | tf_op jit(solution)/shard_map/all_gather | solution.py:70
  93.0 3.9 %convolution_convert_fusion.3 = bf16[128,1024]{1,0:T(8,128)(2,1)S(1)} fusion(bf16[1024,2048]{1,0:T(8,128)(2,1)} %all-gather.4.cloned.1.call-done, bf16[2048,64]{0,1:T(8,128)(2,1)} %param.37, bf16[2048,64]{0,1:T(8,128)(2,1)} %param.25), kind=kOutput, calls=%fused_computation.16 | convolution fusion | flops 538050560 | bytes 4980736 | tf_op jit(solution)/shard_map/rd,dc->cr/dot_general | solution.py:68
  96.9 2.2 collective-permute-start.2
  99.1 1.0 collective-permute-done.2
  100.2 3.0 collective-permute-start.3
  103.3 3.7 collective-permute-done.3
  107.0 0.7 slice_bitcast_fusion.9
  107.7 0.7 pad_maximum_fusion
  108.7 18.7 %all_gather.18 = bf16[128,2048]{1,0:T(8,128)(2,1)S(1)} all-gather(bf16[8,2048]{1,0:T(8,128)(2,1)S(1)} %fusion.52), channel_id=1, replica_groups=mesh['grp'=2,'sp'=16,'tp'=16] {'tp'}, dimensions={0}, use_global_device_ids=true | all-gather | bytes 557056 | tf_op jit(solution)/shard_map/all_gather | solution.py:52
  127.7 2.1 collective-permute-start
  129.8 1.0 collective-permute-done
  130.9 2.0 collective-permute-start.1
  132.8 3.5 collective-permute-done.1
  136.4 41.9 %all-gather.6.cloned.1.call-done = bf16[256,4096]{1,0:T(8,128)(2,1)} async-done(((bf16[256,256]{1,0:T(8,128)(2,1)}), bf16[256,4096]{1,0:T(8,128)(2,1)}) %all-gather.6.cloned.1.call-update) | async-done | bytes 2097168 | tf_op jit(solution)/shard_map/all_gather | solution.py:33
  178.3 2.7 multiply_reduce_fusion.1
  181.1 1.5 fusion
  182.7 13.7 %collective-permute-start.4 = (bf16[128,4]{0,1:T(4,128)(2,1)S(1)}, bf16[128,4]{0,1:T(4,128)(2,1)S(1)}, u32[]{:S(2)}, u32[]{:S(2)}) collective-permute-start(bf16[128,4]{0,1:T(4,128)(2,1)S(1)} %get-tuple-element.43), channel_id=1, source_target_pairs={{0,1},{1,0},{2,3},{3,2},{4,5},{5,4},{6,7},{7,6},{8,9},{9,8},{10,11... | collective-permute-start | bytes 3080 | tf_op jit(solution)/shard_map/ppermute | solution.py:28
  196.4 2.0 collective-permute-start.8
  198.4 3.5 collective-permute-start.6
  201.9 2.0 collective-permute-start.9
  203.9 2.4 collective-permute-done.9
  206.2 0.6 multiply_add_fusion.6
  206.8 2.3 fusion.109
  209.2 4.0 %collective-permute-start.5 = (bf16[128,4,128]{2,0,1:T(8,128)(2,1)}, bf16[128,4,128]{2,0,1:T(8,128)(2,1)}, u32[]{:S(2)}, u32[]{:S(2)}) collective-permute-start(bf16[128,4,128]{2,0,1:T(8,128)(2,1)} %get-tuple-element.47), channel_id=1, source_target_pairs={{0,1},{1,0},{2,3},{3,2},{4,5},{5,4},{6,7},{7,6},{8,9},{9,8},{10,11... | collective-permute-start | bytes 393224 | tf_op jit(solution)/shard_map/ppermute | solution.py:28
  213.2 1.3 collective-permute-done.5
  214.5 1.1 fusion.104
  215.6 2.0 collective-permute-start.7
  217.5 0.7 fusion.84
  218.2 4.0 %collective-permute-done.7 = bf16[128,4,128]{2,0,1:T(8,128)(2,1)S(1)} collective-permute-done((bf16[128,4,128]{2,0,1:T(8,128)(2,1)S(1)}, bf16[128,4,128]{2,0,1:T(8,128)(2,1)S(1)}, u32[]{:S(2)}, u32[]{:S(2)}) %collective-permute-start.7) | collective-permute-done | bytes 131104 | tf_op jit(solution)/shard_map/ppermute | solution.py:28
  222.2 1.2 fusion.8
  223.4 6.5 %all-to-all-start = ((bf16[16,8,2048]{2,1,0:T(8,128)(2,1)}), bf16[16,8,2048]{2,1,0:T(8,128)(2,1)S(1)}, u32[]{:S(2)}, u32[]{:S(2)}) async-start(bf16[16,8,2048]{2,1,0:T(8,128)(2,1)} %fusion.8), calls=%async_computation | async-start | bytes 1048576 | tf_op jit(solution)/shard_map/all_to_all | solution.py:17
  230.0 0.8 fusion.105
  230.8 0.8 fusion.106
  231.6 1.5 pad_maximum_fusion.1
  233.2 13.9 %all-to-all-done = bf16[16,8,2048]{2,1,0:T(8,128)(2,1)S(1)} async-done(((bf16[16,8,2048]{2,1,0:T(8,128)(2,1)}), bf16[16,8,2048]{2,1,0:T(8,128)(2,1)S(1)}, u32[]{:S(2)}, u32[]{:S(2)}) %all-to-all-start) | async-done | bytes 524320 | tf_op jit(solution)/shard_map/all_to_all | solution.py:17
  247.6 16.0 %all_gather.21 = bf16[128,2048]{1,0:T(8,128)(2,1)S(1)} all-gather(bf16[8,2048]{1,0:T(8,128)(2,1)S(1)} %multiply_convert_fusion.1), channel_id=1, replica_groups=mesh['grp'=2,'sp'=16,'tp'=16] {'tp'}, dimensions={0}, use_global_device_ids=true | all-gather | bytes 557056 | tf_op jit(solution)/shard_map/all_gather | solution.py:52
  263.6 0.4 convolution_convert_fusion.5
  264.1 3.2 collective-permute-start.10
  267.8 2.1 collective-permute-start.11
  270.0 1.0 collective-permute-done.11
  271.1 0.6 fusion.9
  271.7 23.3 %all_to_all.15 = bf16[16,8,2048]{2,1,0:T(8,128)(2,1)S(1)} all-to-all(bf16[16,8,2048]{2,1,0:T(8,128)(2,1)S(1)} %fusion.9), channel_id=1, replica_groups=mesh['grp'=2,'sp'=16,'tp'=16] {'tp'}, dimensions={0} | all-to-all | bytes 1048576 | tf_op jit(solution)/shard_map/all_to_all | solution.py:17
  295.6 16.0 %all_gather.22 = bf16[128,2048]{1,0:T(8,128)(2,1)S(1)} all-gather(bf16[8,2048]{1,0:T(8,128)(2,1)S(1)} %multiply_convert_fusion), channel_id=1, replica_groups=mesh['grp'=2,'sp'=16,'tp'=16] {'tp'}, dimensions={0}, use_global_device_ids=true | all-gather | bytes 557056 | tf_op jit(solution)/shard_map/all_gather | solution.py:52
  311.9 2.1 collective-permute-start.12
  314.0 1.0 collective-permute-done.12
  315.1 2.2 collective-permute-start.13
  317.3 3.2 collective-permute-done.13
  320.5 2.7 multiply_reduce_fusion
  323.2 1.5 fusion.2
  324.7 3.0 collective-permute-start.14
  327.7 2.0 collective-permute-start.18
  329.7 2.2 collective-permute-start.16
  331.9 3.2 collective-permute-start.19
  335.1 1.2 collective-permute-done.19
  336.3 1.7 fusion.110
  338.0 3.9 %collective-permute-start.15 = (bf16[128,4,128]{2,0,1:T(8,128)(2,1)S(1)}, bf16[128,4,128]{2,0,1:T(8,128)(2,1)S(1)}, u32[]{:S(2)}, u32[]{:S(2)}) collective-permute-start(bf16[128,4,128]{2,0,1:T(8,128)(2,1)S(1)} %get-tuple-element.51), channel_id=1, source_target_pairs={{0,1},{1,0},{2,3},{3,2},{4,5},{5,4},{6,7},{7,6},{8,9},{9,8},{10,11... | collective-permute-start | bytes 393224 | tf_op jit(solution)/shard_map/ppermute | solution.py:28
  341.9 0.9 collective-permute-done.15
  343.0 3.2 collective-permute-start.17
  346.2 3.4 collective-permute-done.17
  349.6 0.4 fusion.10
  350.0 23.3 %all_to_all.16 = bf16[16,8,2048]{2,1,0:T(8,128)(2,1)S(1)} all-to-all(bf16[16,8,2048]{2,1,0:T(8,128)(2,1)S(1)} %fusion.10), channel_id=1, replica_groups=mesh['grp'=2,'sp'=16,'tp'=16] {'tp'}, dimensions={0} | all-to-all | bytes 1048576 | tf_op jit(solution)/shard_map/all_to_all | solution.py:17
  373.5 0.7 multiply_add_fusion.2
  (92 shorter events, 3.9 us)
Async XLA Ops:
  6.5 264.6 %copy-start = (bf16[176,2048]{1,0:T(8,128)(2,1)S(1)}, bf16[176,2048]{1,0:T(8,128)(2,1)}, u32[]{:S(2)}) copy-start(bf16[176,2048]{1,0:T(8,128)(2,1)} %param.33) | copy-start | bytes 2162692
  6.6 101.9 %copy-start.1 = (bf16[8,2048]{1,0:T(8,128)(2,1)S(1)}, bf16[8,2048]{1,0:T(8,128)(2,1)}, u32[]{:S(2)}) copy-start(bf16[8,2048]{1,0:T(8,128)(2,1)} %param.20) | copy-start | bytes 98308
  6.6 102.0 %copy-start.11 = (f32[2048]{0:T(1024)S(1)}, f32[2048]{0:T(1024)}, u32[]{:S(2)}) copy-start(f32[2048]{0:T(1024)} %param.23) | copy-start | bytes 24580
  6.6 120.8 %copy-start.4 = (bf16[2048,128]{1,0:T(8,128)(2,1)S(1)}, bf16[2048,128]{1,0:T(8,128)(2,1)}, u32[]{:S(2)}) copy-start(bf16[2048,128]{1,0:T(8,128)(2,1)} %param.24) | copy-start | bytes 1572868
  6.6 86.4 %all-gather.4.cloned.1.call-start = ((), (), s32[]{:S(2)}) async-start(), calls=%async_computation.3 | async-start | bytes 4456448 | tf_op jit(solution)/shard_map/all_gather | solution.py:70
  9.7 168.6 %all-gather.6.cloned.1.call-start = ((), (), s32[]{:S(2)}) async-start(), calls=%async_computation.4 | async-start | bytes 2228224 | tf_op jit(solution)/shard_map/all_gather | solution.py:33
  96.9 3.3 collective-permute-start.2
  100.2 6.7 %collective-permute-start.3 = (bf16[2,128,256]{2,1,0:T(8,128)(2,1)S(1)}, bf16[2,128,256]{2,1,0:T(8,128)(2,1)S(1)}, u32[]{:S(2)}, u32[]{:S(2)}) collective-permute-start(bf16[2,128,256]{2,1,0:T(8,128)(2,1)S(1)} %get-tuple-element.30), channel_id=1, source_target_pairs={{0,2},{2,0},{1,3},{3,1},{4,6},{6,4},{5,7},{7,5},{8,10},{10,8},{9,1... | collective-permute-start | bytes 393224 | tf_op jit(solution)/shard_map/ppermute | solution.py:28
  127.7 3.1 collective-permute-start
  130.9 5.5 %collective-permute-start.1 = (bf16[128,256]{0,1:T(8,128)(2,1)S(1)}, bf16[128,256]{0,1:T(8,128)(2,1)S(1)}, u32[]{:S(2)}, u32[]{:S(2)}) collective-permute-start(bf16[128,256]{0,1:T(8,128)(2,1)S(1)} %maximum_select_fusion.7), channel_id=1, source_target_pairs={{0,2},{2,0},{1,3},{3,1},{4,6},{6,4},{5,7},{7,5},{8,10},{10,8},{9,1... | collective-permute-start | bytes 196616 | tf_op jit(solution)/shard_map/ppermute | solution.py:28
  178.3 28.5 %copy-start.9 = (bf16[256,4096]{1,0:T(8,128)(2,1)S(1)}, bf16[256,4096]{1,0:T(8,128)(2,1)}, u32[]{:S(2)}) copy-start(bf16[256,4096]{1,0:T(8,128)(2,1)} %all-gather.6.cloned.1.call-done) | copy-start | bytes 6291460
  181.1 41.1 %copy-start.5 = (bf16[128,2048]{1,0:T(8,128)(2,1)S(1)}, bf16[128,2048]{1,0:T(8,128)(2,1)}, u32[]{:S(2)}) copy-start(bf16[128,2048]{1,0:T(8,128)(2,1)} %param.26) | copy-start | bytes 1572868
  182.6 64.7 %copy-start.10 = (f32[2048]{0:T(1024)S(1)}, f32[2048]{0:T(1024)}, u32[]{:S(2)}) copy-start(f32[2048]{0:T(1024)} %param.27) | copy-start | bytes 24580
  182.6 64.9 %copy-start.12 = (f32[2048]{0:T(1024)S(1)}, f32[2048]{0:T(1024)}, u32[]{:S(2)}) copy-start(f32[2048]{0:T(1024)} %param.28) | copy-start | bytes 24580
  182.6 81.0 %copy-start.2 = (bf16[2048,176]{0,1:T(8,128)(2,1)S(1)}, bf16[2048,176]{0,1:T(8,128)(2,1)}, u32[]{:S(2)}) copy-start(bf16[2048,176]{0,1:T(8,128)(2,1)} %param.29) | copy-start | bytes 2162692
  182.6 84.7 %copy-start.3 = (bf16[2048,176]{0,1:T(8,128)(2,1)S(1)}, bf16[2048,176]{0,1:T(8,128)(2,1)}, u32[]{:S(2)}) copy-start(bf16[2048,176]{0,1:T(8,128)(2,1)} %param.30) | copy-start | bytes 2162692
  182.7 15.7 %collective-permute-start.4 = (bf16[128,4]{0,1:T(4,128)(2,1)S(1)}, bf16[128,4]{0,1:T(4,128)(2,1)S(1)}, u32[]{:S(2)}, u32[]{:S(2)}) collective-permute-start(bf16[128,4]{0,1:T(4,128)(2,1)S(1)} %get-tuple-element.43), channel_id=1, source_target_pairs={{0,1},{1,0},{2,3},{3,2},{4,5},{5,4},{6,7},{7,6},{8,9},{9,8},{10,11... | collective-permute-start | bytes 3080 | tf_op jit(solution)/shard_map/ppermute | solution.py:28
  196.4 5.5 %collective-permute-start.8 = (bf16[128,4]{0,1:T(4,128)(2,1)S(1)}, bf16[128,4]{0,1:T(4,128)(2,1)S(1)}, u32[]{:S(2)}, u32[]{:S(2)}) collective-permute-start(bf16[128,4]{0,1:T(4,128)(2,1)S(1)} %get-tuple-element.44), channel_id=1, source_target_pairs={{0,1},{1,0},{2,3},{3,2},{4,5},{5,4},{6,7},{7,6},{8,9},{9,8},{10,11... | collective-permute-start | bytes 3080 | tf_op jit(solution)/shard_map/ppermute | solution.py:28
  198.4 5.5 %collective-permute-start.6 = (bf16[128,4]{0,1:T(4,128)(2,1)S(1)}, bf16[128,4]{0,1:T(4,128)(2,1)S(1)}, u32[]{:S(2)}, u32[]{:S(2)}) collective-permute-start(bf16[128,4]{0,1:T(4,128)(2,1)S(1)} %fusion.82), channel_id=1, source_target_pairs={{0,2},{2,0},{1,3},{3,1},{4,6},{6,4},{5,7},{7,5},{8,10},{10,8},{9,1... | collective-permute-start | bytes 3080 | tf_op jit(solution)/shard_map/ppermute | solution.py:28
  201.9 4.3 %collective-permute-start.9 = (bf16[128,4]{0,1:T(4,128)(2,1)S(1)}, bf16[128,4]{0,1:T(4,128)(2,1)S(1)}, u32[]{:S(2)}, u32[]{:S(2)}) collective-permute-start(bf16[128,4]{0,1:T(4,128)(2,1)S(1)} %get-tuple-element.19), channel_id=1, source_target_pairs={{0,2},{2,0},{1,3},{3,1},{4,6},{6,4},{5,7},{7,5},{8,10},{10,8},{9,1... | collective-permute-start | bytes 3080 | tf_op jit(solution)/shard_map/ppermute | solution.py:28
  206.8 88.4 %copy-start.13 = (f32[2048]{0:T(1024)S(1)}, f32[2048]{0:T(1024)}, u32[]{:S(2)}) copy-start(f32[2048]{0:T(1024)} %param.34) | copy-start | bytes 24580
  206.8 88.7 %copy-start.15 = (f32[2048]{0:T(1024)S(1)}, f32[2048]{0:T(1024)}, u32[]{:S(2)}) copy-start(f32[2048]{0:T(1024)} %param.35) | copy-start | bytes 24580
  209.2 102.4 %copy-start.6 = (bf16[2048,128]{1,0:T(8,128)(2,1)S(1)}, bf16[2048,128]{1,0:T(8,128)(2,1)}, u32[]{:S(2)}) copy-start(bf16[2048,128]{1,0:T(8,128)(2,1)} %param.36) | copy-start | bytes 1572868
  209.2 5.3 %collective-permute-start.5 = (bf16[128,4,128]{2,0,1:T(8,128)(2,1)}, bf16[128,4,128]{2,0,1:T(8,128)(2,1)}, u32[]{:S(2)}, u32[]{:S(2)}) collective-permute-start(bf16[128,4,128]{2,0,1:T(8,128)(2,1)} %get-tuple-element.47), channel_id=1, source_target_pairs={{0,1},{1,0},{2,3},{3,2},{4,5},{5,4},{6,7},{7,6},{8,9},{9,8},{10,11... | collective-permute-start | bytes 393224 | tf_op jit(solution)/shard_map/ppermute | solution.py:28
  215.6 6.6 %collective-permute-start.7 = (bf16[128,4,128]{2,0,1:T(8,128)(2,1)S(1)}, bf16[128,4,128]{2,0,1:T(8,128)(2,1)S(1)}, u32[]{:S(2)}, u32[]{:S(2)}) collective-permute-start(bf16[128,4,128]{2,0,1:T(8,128)(2,1)S(1)} %get-tuple-element.23), channel_id=1, source_target_pairs={{0,2},{2,0},{1,3},{3,1},{4,6},{6,4},{5,7},{7,5},{8,10},{10,8},{9,1... | collective-permute-start | bytes 393224 | tf_op jit(solution)/shard_map/ppermute | solution.py:28
  223.4 23.7 %all-to-all-start = ((bf16[16,8,2048]{2,1,0:T(8,128)(2,1)}), bf16[16,8,2048]{2,1,0:T(8,128)(2,1)S(1)}, u32[]{:S(2)}, u32[]{:S(2)}) async-start(bf16[16,8,2048]{2,1,0:T(8,128)(2,1)} %fusion.8), calls=%async_computation | async-start | bytes 1048576 | tf_op jit(solution)/shard_map/all_to_all | solution.py:17
  229.9 87.4 %all-gather.8.cloned.1.call-start = ((), (), s32[]{:S(2)}) async-start(), calls=%async_computation.5 | async-start | bytes 2228224 | tf_op jit(solution)/shard_map/all_gather | solution.py:33
  264.1 5.8 %collective-permute-start.10 = (bf16[2,176]{0,1:T(8,128)(2,1)S(1)}, bf16[2,176]{0,1:T(8,128)(2,1)S(1)}, u32[]{:S(2)}, u32[]{:S(2)}) collective-permute-start(bf16[2,176]{0,1:T(8,128)(2,1)S(1)} %slice.122), channel_id=1, source_target_pairs={{0,16},{16,32},{32,48},{48,64},{64,80},{80,96},{96,112},{112,128},... | collective-permute-start | bytes 2120 | tf_op jit(solution)/shard_map/ppermute | solution.py:43
  267.8 3.2 collective-permute-start.11
  311.9 3.1 collective-permute-start.12
  315.1 5.4 %collective-permute-start.13 = (bf16[128,256]{0,1:T(8,128)(2,1)S(1)}, bf16[128,256]{0,1:T(8,128)(2,1)S(1)}, u32[]{:S(2)}, u32[]{:S(2)}) collective-permute-start(bf16[128,256]{0,1:T(8,128)(2,1)S(1)} %maximum_select_fusion.9), channel_id=1, source_target_pairs={{0,2},{2,0},{1,3},{3,1},{4,6},{6,4},{5,7},{7,5},{8,10},{10,8},{9,1... | collective-permute-start | bytes 196616 | tf_op jit(solution)/shard_map/ppermute | solution.py:28
  320.5 15.8 %copy-start.8 = (bf16[256,4096]{1,0:T(8,128)(2,1)S(1)}, bf16[256,4096]{1,0:T(8,128)(2,1)}, u32[]{:S(2)}) copy-start(bf16[256,4096]{1,0:T(8,128)(2,1)} %all-gather.8.cloned.1.call-done) | copy-start | bytes 6291460
  323.2 26.4 %copy-start.7 = (bf16[128,2048]{1,0:T(8,128)(2,1)S(1)}, bf16[128,2048]{1,0:T(8,128)(2,1)}, u32[]{:S(2)}) copy-start(bf16[128,2048]{1,0:T(8,128)(2,1)} %param.38) | copy-start | bytes 1572868
  324.7 48.8 %copy-start.14 = (f32[2048]{0:T(1024)S(1)}, f32[2048]{0:T(1024)}, u32[]{:S(2)}) copy-start(f32[2048]{0:T(1024)} %param.39) | copy-start | bytes 24580
  324.7 4.9 %collective-permute-start.14 = (bf16[128,4]{0,1:T(4,128)(2,1)S(1)}, bf16[128,4]{0,1:T(4,128)(2,1)S(1)}, u32[]{:S(2)}, u32[]{:S(2)}) collective-permute-start(bf16[128,4]{0,1:T(4,128)(2,1)S(1)} %get-tuple-element.40), channel_id=1, source_target_pairs={{0,1},{1,0},{2,3},{3,2},{4,5},{5,4},{6,7},{7,6},{8,9},{9,8},{10,11... | collective-permute-start | bytes 3080 | tf_op jit(solution)/shard_map/ppermute | solution.py:28
  327.7 4.2 %collective-permute-start.18 = (bf16[128,4]{0,1:T(4,128)(2,1)S(1)}, bf16[128,4]{0,1:T(4,128)(2,1)S(1)}, u32[]{:S(2)}, u32[]{:S(2)}) collective-permute-start(bf16[128,4]{0,1:T(4,128)(2,1)S(1)} %get-tuple-element.41), channel_id=1, source_target_pairs={{0,1},{1,0},{2,3},{3,2},{4,5},{5,4},{6,7},{7,6},{8,9},{9,8},{10,11... | collective-permute-start | bytes 3080 | tf_op jit(solution)/shard_map/ppermute | solution.py:28
  329.7 5.4 %collective-permute-start.16 = (bf16[128,4]{0,1:T(4,128)(2,1)S(1)}, bf16[128,4]{0,1:T(4,128)(2,1)S(1)}, u32[]{:S(2)}, u32[]{:S(2)}) collective-permute-start(bf16[128,4]{0,1:T(4,128)(2,1)S(1)} %fusion.83), channel_id=1, source_target_pairs={{0,2},{2,0},{1,3},{3,1},{4,6},{6,4},{5,7},{7,5},{8,10},{10,8},{9,1... | collective-permute-start | bytes 3080 | tf_op jit(solution)/shard_map/ppermute | solution.py:28
  331.9 4.3 %collective-permute-start.19 = (bf16[128,4]{0,1:T(4,128)(2,1)S(1)}, bf16[128,4]{0,1:T(4,128)(2,1)S(1)}, u32[]{:S(2)}, u32[]{:S(2)}) collective-permute-start(bf16[128,4]{0,1:T(4,128)(2,1)S(1)} %get-tuple-element.8), channel_id=1, source_target_pairs={{0,2},{2,0},{1,3},{3,1},{4,6},{6,4},{5,7},{7,5},{8,10},{10,8},{9,1... | collective-permute-start | bytes 3080 | tf_op jit(solution)/shard_map/ppermute | solution.py:28
  338.0 4.8 %collective-permute-start.15 = (bf16[128,4,128]{2,0,1:T(8,128)(2,1)S(1)}, bf16[128,4,128]{2,0,1:T(8,128)(2,1)S(1)}, u32[]{:S(2)}, u32[]{:S(2)}) collective-permute-start(bf16[128,4,128]{2,0,1:T(8,128)(2,1)S(1)} %get-tuple-element.51), channel_id=1, source_target_pairs={{0,1},{1,0},{2,3},{3,2},{4,5},{5,4},{6,7},{7,6},{8,9},{9,8},{10,11... | collective-permute-start | bytes 393224 | tf_op jit(solution)/shard_map/ppermute | solution.py:28
  343.0 6.6 %collective-permute-start.17 = (bf16[128,4,128]{2,0,1:T(8,128)(2,1)S(1)}, bf16[128,4,128]{2,0,1:T(8,128)(2,1)S(1)}, u32[]{:S(2)}, u32[]{:S(2)}) collective-permute-start(bf16[128,4,128]{2,0,1:T(8,128)(2,1)S(1)} %get-tuple-element.12), channel_id=1, source_target_pairs={{0,2},{2,0},{1,3},{3,1},{4,6},{6,4},{5,7},{7,5},{8,10},{10,8},{9,1... | collective-permute-start | bytes 393224 | tf_op jit(solution)/shard_map/ppermute | solution.py:28
Sparse Core Ops, SparseCore 0:
  9.8 83.0 all-gather.3
  108.6 69.7 all-gather.5
  233.3 66.6 all-gather.7
where the time goes:
time: 382 us; the launch traced here: 381 us
  waiting for transfers between devices  167 us (44%)
  blocking collectives  97.2 us (25%)
  starting transfers between devices  70 us (18%)
  matrix products  16.9 us (4%)
  between operations  13.8 us (4%)
  other arithmetic  12.8 us (3%)
    all_gather x1, waiting for transfers between devices, key_columns(): lax.all_gather(source_rows, 'tp', axis=0, tiled=True)  83.2 us
    ppermute x18, starting transfers between devices, swapped(): return lax.ppermute(block, axis, route)  57.9 us
    all_gather x3, blocking collectives, project_rows(): shard_rows = lax.all_gather(rows_here, 'tp', axis=0, tiled=True)  50.6 us
    all_to_all x2, blocking collectives, sent_and_summed(): lax.all_to_all(parts, axis, split_axis=0, concat_axis=0, tiled=True)  46.6 us
    all_gather x2, waiting for transfers between devices, in_one_piece(): result, at, done = (lax.all_gather(both, axis, axis=dim, tiled=True), 0, [])  42 us
    ppermute x18, waiting for transfers between devices, swapped(): return lax.ppermute(block, axis, route)  26.6 us
    all_to_all x1, waiting for transfers between devices, sent_and_summed(): lax.all_to_all(parts, axis, split_axis=0, concat_axis=0, tiled=True)  13.9 us
  transfers between devices with their start and end apart: 24, of which 16 were waited for; matrix products, arithmetic and copies ran while one was open for 2% of the time, Pallas kernels for 0%

commit v1 on v0

--- a/solution.py
+++ b/solution.py
@@ -5,6 +5,14 @@
 
 HEAD = 128
 KVH = 4
+
+
+def gather_from_all(array, axis, dim):
+    size = lax.axis_size(axis)
+    repeats = [size if d == dim else 1 for d in range(array.ndim)]
+    return lax.all_to_all(
+        jnp.tile(array, repeats), axis, split_axis=dim, concat_axis=dim, tiled=True
+    )
 
 
 def in_blocks(array, dim, size):
@@ -67,7 +75,7 @@
     both_layers = jnp.concatenate([keyval_first, keyval_second], axis=1)
     columns = jnp.einsum(
         "rd,dc->cr",
-        lax.all_gather(source_rows, "tp", axis=0, tiled=True),
+        gather_from_all(source_rows, "tp", 0),
         both_layers,
         preferred_element_type=jnp.float32,
     ).astype(jnp.bfloat16)

time: 382 us -> 436 us (1.14)
  starting transfers between devices: 70 us -> 116 us
  waiting for transfers between devices: 167 us -> 173 us
    all_to_all x0 -> x1, waiting for transfers between devices: none -> 93.6 us  [gather_from_all(): lax.all_to_all(jnp.tile(array, repeats), axis, split_axis=dim, concat_axi...]
    all_gather x1 -> x0, waiting for transfers between devices: 83.2 us -> none  [key_columns(): lax.all_gather(source_rows, 'tp', axis=0, tiled=True)]
    all_to_all x0 -> x1, starting transfers between devices: none -> 45.8 us  [gather_from_all(): lax.all_to_all(jnp.tile(array, repeats), axis, split_axis=dim, concat_axi...]
    all_gather x2, waiting for transfers between devices: 42 us -> 37.6 us  [in_one_piece(): result, at, done = (lax.all_gather(both, axis, axis=dim, tiled=True), 0, [])]
where the time goes in v1:
time: 436 us; the launch traced here: 434 us
  waiting for transfers between devices  173 us (40%)
  starting transfers between devices  116 us (27%)
  blocking collectives  96.6 us (22%)
  matrix products  16.8 us (4%)
  between operations  14.1 us (3%)
  other arithmetic  12.1 us (3%)
  local copies, waits for them, and re-layouts  5.74 us (1%)
    all_to_all x1, waiting for transfers between devices, gather_from_all(): lax.all_to_all(jnp.tile(array, repeats), axis, split_axis=dim, concat_axi...  93.6 us
    ppermute x18, starting transfers between devices, swapped(): return lax.ppermute(block, axis, route)  57.8 us
    all_gather x3, blocking collectives, project_rows(): shard_rows = lax.all_gather(rows_here, 'tp', axis=0, tiled=True)  50 us
    all_to_all x2, blocking collectives, sent_and_summed(): lax.all_to_all(parts, axis, split_axis=0, concat_axis=0, tiled=True)  46.6 us
    all_to_all x1, starting transfers between devices, gather_from_all(): lax.all_to_all(jnp.tile(array, repeats), axis, split_axis=dim, concat_axi...  45.8 us
    all_gather x2, waiting for transfers between devices, in_one_piece(): result, at, done = (lax.all_gather(both, axis, axis=dim, tiled=True), 0, [])  37.6 us
    ppermute x18, waiting for transfers between devices, swapped(): return lax.ppermute(block, axis, route)  26.7 us
    all_to_all x1, waiting for transfers between devices, sent_and_summed(): lax.all_to_all(parts, axis, split_axis=0, concat_axis=0, tiled=True)  13.9 us
  transfers between devices with their start and end apart: 24, of which 16 were waited for; matrix products, arithmetic and copies ran while one was open for 2% of the time, Pallas kernels for 0%

profile of v1, /device:TPU:65, one launch (start us, length us, event | category | flops | bytes accessed | tf_op | source)
XLA Modules:
  0.0 434.4 jit_solution(17654874919762111300)
XLA Ops:
  6.6 1.2 fusion.19
  7.8 1.1 fusion.21
  8.9 2.5 tile.2
  11.4 45.8 %all-to-all-start = ((bf16[16,64,2048]{2,1,0:T(8,128)(2,1)}), bf16[16,64,2048]{2,1,0:T(8,128)(2,1)}, u32[]{:S(2)}, u32[]{:S(2)}) async-start(bf16[16,64,2048]{2,1,0:T(8,128)(2,1)} %tile.2), calls=%async_computation | async-start | bytes 8388608 | tf_op jit(solution)/shard_map/all_to_all | solution.py:13
  57.3 93.6 %all-to-all-done = bf16[16,64,2048]{2,1,0:T(8,128)(2,1)} async-done(((bf16[16,64,2048]{2,1,0:T(8,128)(2,1)}), bf16[16,64,2048]{2,1,0:T(8,128)(2,1)}, u32[]{:S(2)}, u32[]{:S(2)}) %all-to-all-start) | async-done | bytes 4194336 | tf_op jit(solution)/shard_map/all_to_all | solution.py:13
  151.0 3.7 convolution_convert_fusion.3
  154.7 2.9 collective-permute-start.2
  157.6 0.9 collective-permute-done.2
  158.7 2.0 collective-permute-start.3
  160.6 4.7 %collective-permute-done.3 = bf16[2,128,256]{2,1,0:T(8,128)(2,1)S(1)} collective-permute-done((bf16[2,128,256]{2,1,0:T(8,128)(2,1)S(1)}, bf16[2,128,256]{2,1,0:T(8,128)(2,1)S(1)}, u32[]{:S(2)}, u32[]{:S(2)}) %collective-permute-start.3) | collective-permute-done | bytes 131104 | tf_op jit(solution)/shard_map/ppermute | solution.py:36
  165.4 0.7 slice_bitcast_fusion.9
  166.1 0.7 pad_maximum_fusion
  167.0 18.1 %all_gather.15 = bf16[128,2048]{1,0:T(8,128)(2,1)S(1)} all-gather(bf16[8,2048]{1,0:T(8,128)(2,1)S(1)} %fusion.52), channel_id=1, replica_groups=mesh['grp'=2,'sp'=16,'tp'=16] {'tp'}, dimensions={0}, use_global_device_ids=true | all-gather | bytes 557056 | tf_op jit(solution)/shard_map/all_gather | solution.py:60
  185.5 2.1 collective-permute-start
  187.6 1.0 collective-permute-done
  188.6 2.2 collective-permute-start.1
  190.9 3.3 collective-permute-done.1
  194.1 37.5 %all-gather.3.cloned.1.call-done = bf16[256,4096]{1,0:T(8,128)(2,1)} async-done(((bf16[256,256]{1,0:T(8,128)(2,1)}), bf16[256,4096]{1,0:T(8,128)(2,1)}) %all-gather.3.cloned.1.call-update) | async-done | bytes 2097168 | tf_op jit(solution)/shard_map/all_gather | solution.py:41
  231.7 2.7 multiply_reduce_fusion.1
  234.4 1.5 fusion
  236.0 13.6 %collective-permute-start.4 = (bf16[128,4]{0,1:T(4,128)(2,1)S(1)}, bf16[128,4]{0,1:T(4,128)(2,1)S(1)}, u32[]{:S(2)}, u32[]{:S(2)}) collective-permute-start(bf16[128,4]{0,1:T(4,128)(2,1)S(1)} %get-tuple-element.43), channel_id=1, source_target_pairs={{0,1},{1,0},{2,3},{3,2},{4,5},{5,4},{6,7},{7,6},{8,9},{9,8},{10,11... | collective-permute-start | bytes 3080 | tf_op jit(solution)/shard_map/ppermute | solution.py:36
  249.6 2.0 collective-permute-start.8
  251.6 3.1 collective-permute-start.6
  254.8 2.2 collective-permute-start.9
  257.0 2.1 collective-permute-done.9
  259.1 0.6 multiply_add_fusion.6
  259.7 2.3 fusion.109
  262.0 4.0 collective-permute-start.5
  266.0 1.3 collective-permute-done.5
  267.3 1.1 fusion.104
  268.4 2.2 collective-permute-start.7
  270.6 0.7 fusion.84
  271.3 3.7 collective-permute-done.7
  275.1 1.2 fusion.8
  276.2 7.0 %all-to-all-start.1 = ((bf16[16,8,2048]{2,1,0:T(8,128)(2,1)}), bf16[16,8,2048]{2,1,0:T(8,128)(2,1)S(1)}, u32[]{:S(2)}, u32[]{:S(2)}) async-start(bf16[16,8,2048]{2,1,0:T(8,128)(2,1)} %fusion.8), calls=%async_computation.1 | async-start | bytes 1048576 | tf_op jit(solution)/shard_map/all_to_all | solution.py:25
  283.3 0.8 fusion.105
  284.1 0.8 fusion.106
  284.9 1.5 pad_maximum_fusion.1
  286.5 13.9 %all-to-all-done.1 = bf16[16,8,2048]{2,1,0:T(8,128)(2,1)S(1)} async-done(((bf16[16,8,2048]{2,1,0:T(8,128)(2,1)}), bf16[16,8,2048]{2,1,0:T(8,128)(2,1)S(1)}, u32[]{:S(2)}, u32[]{:S(2)}) %all-to-all-start.1) | async-done | bytes 524320 | tf_op jit(solution)/shard_map/all_to_all | solution.py:25
  301.0 16.0 %all_gather.17 = bf16[128,2048]{1,0:T(8,128)(2,1)S(1)} all-gather(bf16[8,2048]{1,0:T(8,128)(2,1)S(1)} %multiply_convert_fusion.1), channel_id=1, replica_groups=mesh['grp'=2,'sp'=16,'tp'=16] {'tp'}, dimensions={0}, use_global_device_ids=true | all-gather | bytes 557056 | tf_op jit(solution)/shard_map/all_gather | solution.py:60
  317.4 3.0 collective-permute-start.10
  320.9 2.5 collective-permute-start.11
  323.5 0.8 collective-permute-done.11
  324.5 0.6 fusion.9
  325.1 23.3 %all_to_all.24 = bf16[16,8,2048]{2,1,0:T(8,128)(2,1)S(1)} all-to-all(bf16[16,8,2048]{2,1,0:T(8,128)(2,1)S(1)} %fusion.9), channel_id=1, replica_groups=mesh['grp'=2,'sp'=16,'tp'=16] {'tp'}, dimensions={0} | all-to-all | bytes 1048576 | tf_op jit(solution)/shard_map/all_to_all | solution.py:25
  348.9 16.0 %all_gather.18 = bf16[128,2048]{1,0:T(8,128)(2,1)S(1)} all-gather(bf16[8,2048]{1,0:T(8,128)(2,1)S(1)} %multiply_convert_fusion), channel_id=1, replica_groups=mesh['grp'=2,'sp'=16,'tp'=16] {'tp'}, dimensions={0}, use_global_device_ids=true | all-gather | bytes 557056 | tf_op jit(solution)/shard_map/all_gather | solution.py:60
  365.2 2.1 collective-permute-start.12
  367.4 1.0 collective-permute-done.12
  368.4 2.2 collective-permute-start.13
  370.6 3.2 collective-permute-done.13
  373.8 2.7 multiply_reduce_fusion
  376.6 1.5 fusion.2
  378.1 3.0 collective-permute-start.14
  381.1 2.0 collective-permute-start.18
  383.0 2.2 collective-permute-start.16
  385.3 3.2 collective-permute-start.19
  388.4 1.2 collective-permute-done.19
  389.6 1.7 fusion.110
  391.3 3.9 collective-permute-start.15
  395.2 0.9 collective-permute-done.15
  396.4 3.2 collective-permute-start.17
  399.6 3.4 collective-permute-done.17
  403.4 23.3 %all_to_all.25 = bf16[16,8,2048]{2,1,0:T(8,128)(2,1)S(1)} all-to-all(bf16[16,8,2048]{2,1,0:T(8,128)(2,1)S(1)} %fusion.10), channel_id=1, replica_groups=mesh['grp'=2,'sp'=16,'tp'=16] {'tp'}, dimensions={0} | all-to-all | bytes 1048576 | tf_op jit(solution)/shard_map/all_to_all | solution.py:25
  426.9 0.7 multiply_add_fusion.2
  (96 shorter events, 4.5 us)
Async XLA Ops:
  6.5 317.9 %copy-start = (bf16[176,2048]{1,0:T(8,128)(2,1)S(1)}, bf16[176,2048]{1,0:T(8,128)(2,1)}, u32[]{:S(2)}) copy-start(bf16[176,2048]{1,0:T(8,128)(2,1)} %param.33) | copy-start | bytes 2162692
  6.6 144.4 %copy-start.11 = (bf16[2048,64]{0,1:T(8,128)(2,1)S(1)}, bf16[2048,64]{0,1:T(8,128)(2,1)}, u32[]{:S(2)}) copy-start(bf16[2048,64]{0,1:T(8,128)(2,1)} %param.25) | copy-start | bytes 786436
  6.6 144.4 %copy-start.10 = (bf16[2048,64]{0,1:T(8,128)(2,1)S(1)}, bf16[2048,64]{0,1:T(8,128)(2,1)}, u32[]{:S(2)}) copy-start(bf16[2048,64]{0,1:T(8,128)(2,1)} %param.37) | copy-start | bytes 786436
  11.4 155.4 %copy-start.1 = (bf16[8,2048]{1,0:T(8,128)(2,1)S(1)}, bf16[8,2048]{1,0:T(8,128)(2,1)}, u32[]{:S(2)}) copy-start(bf16[8,2048]{1,0:T(8,128)(2,1)} %param.20) | copy-start | bytes 98308
  11.4 155.5 %copy-start.13 = (f32[2048]{0:T(1024)S(1)}, f32[2048]{0:T(1024)}, u32[]{:S(2)}) copy-start(f32[2048]{0:T(1024)} %param.23) | copy-start | bytes 24580
  11.4 173.7 %copy-start.4 = (bf16[2048,128]{1,0:T(8,128)(2,1)S(1)}, bf16[2048,128]{1,0:T(8,128)(2,1)}, u32[]{:S(2)}) copy-start(bf16[2048,128]{1,0:T(8,128)(2,1)} %param.24) | copy-start | bytes 1572868
  11.4 139.6 %all-to-all-start = ((bf16[16,64,2048]{2,1,0:T(8,128)(2,1)}), bf16[16,64,2048]{2,1,0:T(8,128)(2,1)}, u32[]{:S(2)}, u32[]{:S(2)}) async-start(bf16[16,64,2048]{2,1,0:T(8,128)(2,1)} %tile.2), calls=%async_computation | async-start | bytes 8388608 | tf_op jit(solution)/shard_map/all_to_all | solution.py:13
  57.3 174.4 %all-gather.3.cloned.1.call-start = ((), (), s32[]{:S(2)}) async-start(), calls=%async_computation.4 | async-start | bytes 2228224 | tf_op jit(solution)/shard_map/all_gather | solution.py:41
  154.7 3.9 collective-permute-start.2
  158.7 6.6 %collective-permute-start.3 = (bf16[2,128,256]{2,1,0:T(8,128)(2,1)S(1)}, bf16[2,128,256]{2,1,0:T(8,128)(2,1)S(1)}, u32[]{:S(2)}, u32[]{:S(2)}) collective-permute-start(bf16[2,128,256]{2,1,0:T(8,128)(2,1)S(1)} %get-tuple-element.30), channel_id=1, source_target_pairs={{0,2},{2,0},{1,3},{3,1},{4,6},{6,4},{5,7},{7,5},{8,10},{10,8},{9,1... | collective-permute-start | bytes 393224 | tf_op jit(solution)/shard_map/ppermute | solution.py:36
  185.5 3.1 collective-permute-start
  188.6 5.5 %collective-permute-start.1 = (bf16[128,256]{0,1:T(8,128)(2,1)S(1)}, bf16[128,256]{0,1:T(8,128)(2,1)S(1)}, u32[]{:S(2)}, u32[]{:S(2)}) collective-permute-start(bf16[128,256]{0,1:T(8,128)(2,1)S(1)} %maximum_select_fusion.7), channel_id=1, source_target_pairs={{0,2},{2,0},{1,3},{3,1},{4,6},{6,4},{5,7},{7,5},{8,10},{10,8},{9,1... | collective-permute-start | bytes 196616 | tf_op jit(solution)/shard_map/ppermute | solution.py:36
  231.7 28.0 %copy-start.9 = (bf16[256,4096]{1,0:T(8,128)(2,1)S(1)}, bf16[256,4096]{1,0:T(8,128)(2,1)}, u32[]{:S(2)}) copy-start(bf16[256,4096]{1,0:T(8,128)(2,1)} %all-gather.3.cloned.1.call-done) | copy-start | bytes 6291460
  234.4 40.6 %copy-start.5 = (bf16[128,2048]{1,0:T(8,128)(2,1)S(1)}, bf16[128,2048]{1,0:T(8,128)(2,1)}, u32[]{:S(2)}) copy-start(bf16[128,2048]{1,0:T(8,128)(2,1)} %param.26) | copy-start | bytes 1572868
  235.9 64.7 %copy-start.12 = (f32[2048]{0:T(1024)S(1)}, f32[2048]{0:T(1024)}, u32[]{:S(2)}) copy-start(f32[2048]{0:T(1024)} %param.27) | copy-start | bytes 24580
  236.0 64.9 %copy-start.14 = (f32[2048]{0:T(1024)S(1)}, f32[2048]{0:T(1024)}, u32[]{:S(2)}) copy-start(f32[2048]{0:T(1024)} %param.28) | copy-start | bytes 24580
  236.0 81.0 %copy-start.2 = (bf16[2048,176]{0,1:T(8,128)(2,1)S(1)}, bf16[2048,176]{0,1:T(8,128)(2,1)}, u32[]{:S(2)}) copy-start(bf16[2048,176]{0,1:T(8,128)(2,1)} %param.29) | copy-start | bytes 2162692
  236.0 84.5 %copy-start.3 = (bf16[2048,176]{0,1:T(8,128)(2,1)S(1)}, bf16[2048,176]{0,1:T(8,128)(2,1)}, u32[]{:S(2)}) copy-start(bf16[2048,176]{0,1:T(8,128)(2,1)} %param.30) | copy-start | bytes 2162692
  236.0 15.6 %collective-permute-start.4 = (bf16[128,4]{0,1:T(4,128)(2,1)S(1)}, bf16[128,4]{0,1:T(4,128)(2,1)S(1)}, u32[]{:S(2)}, u32[]{:S(2)}) collective-permute-start(bf16[128,4]{0,1:T(4,128)(2,1)S(1)} %get-tuple-element.43), channel_id=1, source_target_pairs={{0,1},{1,0},{2,3},{3,2},{4,5},{5,4},{6,7},{7,6},{8,9},{9,8},{10,11... | collective-permute-start | bytes 3080 | tf_op jit(solution)/shard_map/ppermute | solution.py:36
  249.6 5.1 %collective-permute-start.8 = (bf16[128,4]{0,1:T(4,128)(2,1)S(1)}, bf16[128,4]{0,1:T(4,128)(2,1)S(1)}, u32[]{:S(2)}, u32[]{:S(2)}) collective-permute-start(bf16[128,4]{0,1:T(4,128)(2,1)S(1)} %get-tuple-element.44), channel_id=1, source_target_pairs={{0,1},{1,0},{2,3},{3,2},{4,5},{5,4},{6,7},{7,6},{8,9},{9,8},{10,11... | collective-permute-start | bytes 3080 | tf_op jit(solution)/shard_map/ppermute | solution.py:36
  251.6 5.4 %collective-permute-start.6 = (bf16[128,4]{0,1:T(4,128)(2,1)S(1)}, bf16[128,4]{0,1:T(4,128)(2,1)S(1)}, u32[]{:S(2)}, u32[]{:S(2)}) collective-permute-start(bf16[128,4]{0,1:T(4,128)(2,1)S(1)} %fusion.82), channel_id=1, source_target_pairs={{0,2},{2,0},{1,3},{3,1},{4,6},{6,4},{5,7},{7,5},{8,10},{10,8},{9,1... | collective-permute-start | bytes 3080 | tf_op jit(solution)/shard_map/ppermute | solution.py:36
  254.8 4.3 %collective-permute-start.9 = (bf16[128,4]{0,1:T(4,128)(2,1)S(1)}, bf16[128,4]{0,1:T(4,128)(2,1)S(1)}, u32[]{:S(2)}, u32[]{:S(2)}) collective-permute-start(bf16[128,4]{0,1:T(4,128)(2,1)S(1)} %get-tuple-element.19), channel_id=1, source_target_pairs={{0,2},{2,0},{1,3},{3,1},{4,6},{6,4},{5,7},{7,5},{8,10},{10,8},{9,1... | collective-permute-start | bytes 3080 | tf_op jit(solution)/shard_map/ppermute | solution.py:36
  259.7 88.9 %copy-start.15 = (f32[2048]{0:T(1024)S(1)}, f32[2048]{0:T(1024)}, u32[]{:S(2)}) copy-start(f32[2048]{0:T(1024)} %param.34) | copy-start | bytes 24580
  259.7 89.2 %copy-start.17 = (f32[2048]{0:T(1024)S(1)}, f32[2048]{0:T(1024)}, u32[]{:S(2)}) copy-start(f32[2048]{0:T(1024)} %param.35) | copy-start | bytes 24580
  262.0 102.9 %copy-start.6 = (bf16[2048,128]{1,0:T(8,128)(2,1)S(1)}, bf16[2048,128]{1,0:T(8,128)(2,1)}, u32[]{:S(2)}) copy-start(bf16[2048,128]{1,0:T(8,128)(2,1)} %param.36) | copy-start | bytes 1572868
  262.0 5.3 %collective-permute-start.5 = (bf16[128,4,128]{2,0,1:T(8,128)(2,1)}, bf16[128,4,128]{2,0,1:T(8,128)(2,1)}, u32[]{:S(2)}, u32[]{:S(2)}) collective-permute-start(bf16[128,4,128]{2,0,1:T(8,128)(2,1)} %get-tuple-element.47), channel_id=1, source_target_pairs={{0,1},{1,0},{2,3},{3,2},{4,5},{5,4},{6,7},{7,6},{8,9},{9,8},{10,11... | collective-permute-start | bytes 393224 | tf_op jit(solution)/shard_map/ppermute | solution.py:36
  268.4 6.6 %collective-permute-start.7 = (bf16[128,4,128]{2,0,1:T(8,128)(2,1)S(1)}, bf16[128,4,128]{2,0,1:T(8,128)(2,1)S(1)}, u32[]{:S(2)}, u32[]{:S(2)}) collective-permute-start(bf16[128,4,128]{2,0,1:T(8,128)(2,1)S(1)} %get-tuple-element.23), channel_id=1, source_target_pairs={{0,2},{2,0},{1,3},{3,1},{4,6},{6,4},{5,7},{7,5},{8,10},{10,8},{9,1... | collective-permute-start | bytes 393224 | tf_op jit(solution)/shard_map/ppermute | solution.py:36
  276.2 24.2 %all-to-all-start.1 = ((bf16[16,8,2048]{2,1,0:T(8,128)(2,1)}), bf16[16,8,2048]{2,1,0:T(8,128)(2,1)S(1)}, u32[]{:S(2)}, u32[]{:S(2)}) async-start(bf16[16,8,2048]{2,1,0:T(8,128)(2,1)} %fusion.8), calls=%async_computation.1 | async-start | bytes 1048576 | tf_op jit(solution)/shard_map/all_to_all | solution.py:25
  283.3 87.4 %all-gather.5.cloned.1.call-start = ((), (), s32[]{:S(2)}) async-start(), calls=%async_computation.5 | async-start | bytes 2228224 | tf_op jit(solution)/shard_map/all_gather | solution.py:41
  317.4 6.0 %collective-permute-start.10 = (bf16[2,176]{0,1:T(8,128)(2,1)S(1)}, bf16[2,176]{0,1:T(8,128)(2,1)S(1)}, u32[]{:S(2)}, u32[]{:S(2)}) collective-permute-start(bf16[2,176]{0,1:T(8,128)(2,1)S(1)} %slice.122), channel_id=1, source_target_pairs={{0,16},{16,32},{32,48},{48,64},{64,80},{80,96},{96,112},{112,128},... | collective-permute-start | bytes 2120 | tf_op jit(solution)/shard_map/ppermute | solution.py:51
  320.9 3.4 collective-permute-start.11
  365.2 3.1 collective-permute-start.12
  368.4 5.4 %collective-permute-start.13 = (bf16[128,256]{0,1:T(8,128)(2,1)S(1)}, bf16[128,256]{0,1:T(8,128)(2,1)S(1)}, u32[]{:S(2)}, u32[]{:S(2)}) collective-permute-start(bf16[128,256]{0,1:T(8,128)(2,1)S(1)} %maximum_select_fusion.9), channel_id=1, source_target_pairs={{0,2},{2,0},{1,3},{3,1},{4,6},{6,4},{5,7},{7,5},{8,10},{10,8},{9,1... | collective-permute-start | bytes 196616 | tf_op jit(solution)/shard_map/ppermute | solution.py:36
  373.8 15.8 %copy-start.8 = (bf16[256,4096]{1,0:T(8,128)(2,1)S(1)}, bf16[256,4096]{1,0:T(8,128)(2,1)}, u32[]{:S(2)}) copy-start(bf16[256,4096]{1,0:T(8,128)(2,1)} %all-gather.5.cloned.1.call-done) | copy-start | bytes 6291460
  376.6 26.4 %copy-start.7 = (bf16[128,2048]{1,0:T(8,128)(2,1)S(1)}, bf16[128,2048]{1,0:T(8,128)(2,1)}, u32[]{:S(2)}) copy-start(bf16[128,2048]{1,0:T(8,128)(2,1)} %param.38) | copy-start | bytes 1572868
  378.1 48.8 %copy-start.16 = (f32[2048]{0:T(1024)S(1)}, f32[2048]{0:T(1024)}, u32[]{:S(2)}) copy-start(f32[2048]{0:T(1024)} %param.39) | copy-start | bytes 24580
  378.1 4.9 %collective-permute-start.14 = (bf16[128,4]{0,1:T(4,128)(2,1)S(1)}, bf16[128,4]{0,1:T(4,128)(2,1)S(1)}, u32[]{:S(2)}, u32[]{:S(2)}) collective-permute-start(bf16[128,4]{0,1:T(4,128)(2,1)S(1)} %get-tuple-element.40), channel_id=1, source_target_pairs={{0,1},{1,0},{2,3},{3,2},{4,5},{5,4},{6,7},{7,6},{8,9},{9,8},{10,11... | collective-permute-start | bytes 3080 | tf_op jit(solution)/shard_map/ppermute | solution.py:36
  381.1 4.2 collective-permute-start.18
  383.0 5.4 %collective-permute-start.16 = (bf16[128,4]{0,1:T(4,128)(2,1)S(1)}, bf16[128,4]{0,1:T(4,128)(2,1)S(1)}, u32[]{:S(2)}, u32[]{:S(2)}) collective-permute-start(bf16[128,4]{0,1:T(4,128)(2,1)S(1)} %fusion.83), channel_id=1, source_target_pairs={{0,2},{2,0},{1,3},{3,1},{4,6},{6,4},{5,7},{7,5},{8,10},{10,8},{9,1... | collective-permute-start | bytes 3080 | tf_op jit(solution)/shard_map/ppermute | solution.py:36
  385.3 4.3 %collective-permute-start.19 = (bf16[128,4]{0,1:T(4,128)(2,1)S(1)}, bf16[128,4]{0,1:T(4,128)(2,1)S(1)}, u32[]{:S(2)}, u32[]{:S(2)}) collective-permute-start(bf16[128,4]{0,1:T(4,128)(2,1)S(1)} %get-tuple-element.8), channel_id=1, source_target_pairs={{0,2},{2,0},{1,3},{3,1},{4,6},{6,4},{5,7},{7,5},{8,10},{10,8},{9,1... | collective-permute-start | bytes 3080 | tf_op jit(solution)/shard_map/ppermute | solution.py:36
  391.3 4.8 %collective-permute-start.15 = (bf16[128,4,128]{2,0,1:T(8,128)(2,1)S(1)}, bf16[128,4,128]{2,0,1:T(8,128)(2,1)S(1)}, u32[]{:S(2)}, u32[]{:S(2)}) collective-permute-start(bf16[128,4,128]{2,0,1:T(8,128)(2,1)S(1)} %get-tuple-element.51), channel_id=1, source_target_pairs={{0,1},{1,0},{2,3},{3,2},{4,5},{5,4},{6,7},{7,6},{8,9},{9,8},{10,11... | collective-permute-start | bytes 393224 | tf_op jit(solution)/shard_map/ppermute | solution.py:36
  396.4 6.6 %collective-permute-start.17 = (bf16[128,4,128]{2,0,1:T(8,128)(2,1)S(1)}, bf16[128,4,128]{2,0,1:T(8,128)(2,1)S(1)}, u32[]{:S(2)}, u32[]{:S(2)}) collective-permute-start(bf16[128,4,128]{2,0,1:T(8,128)(2,1)S(1)} %get-tuple-element.12), channel_id=1, source_target_pairs={{0,2},{2,0},{1,3},{3,1},{4,6},{6,4},{5,7},{7,5},{8,10},{10,8},{9,1... | collective-permute-start | bytes 393224 | tf_op jit(solution)/shard_map/ppermute | solution.py:36
Sparse Core Ops, SparseCore 0:
  166.9 64.7 all-gather.2
  286.6 66.0 all-gather.4
